TPU v7x, 32 devices: a whole 2x2x4 slice. The times are simulated.
32 devices in a mesh: grp: 2 (over y), dp: 2 (over x), kv: 4 (over z), tp: 2 (over core).
Axes of the slice: x: 2, y: 2, z: 4, core: 2. Of those that a mesh axis runs over, the one named last changes fastest.
Arguments:
- resid: bfloat16 [12, 2048], P(('grp', 'dp'), ('kv', 'tp')), parts along dimension 0, may hold values from -7 to 7
- keys_cache: bfloat16 [12, 4096, 256], P(('grp', 'dp'), 'kv', 'tp'), parts along dimension 0, may hold values from -310 to 310
- values_cache: bfloat16 [12, 4096, 256], P(('grp', 'dp'), 'kv', 'tp'), parts along dimension 0, may hold values from -6 to 6
- gates_cache: float32 [12, 4096, 4], P(('grp', 'dp'), 'kv', 'tp'), parts along dimension 0, may hold values from -1044 to 0, as said below
- norm_gain: float32 [2048], replicated, may hold values from 0.1 to 1.9
- w_query: bfloat16 [2048, 2048], P('kv', 'tp'), may hold values from -0.125 to 0.125
- w_key: bfloat16 [2048, 256], P('kv', 'tp'), may hold values from -0.125 to 0.125
- w_value: bfloat16 [2048, 256], P('kv', 'tp'), may hold values from -0.5 to 0.5
- w_forget: bfloat16 [2048, 4], replicated, may hold values from -0.125 to 0.125
- forget_bias: float32 [4], replicated, may hold values from -3 to 1
- w_out: bfloat16 [2048, 2048], P('tp', 'kv'), may hold values from -0.5 to 0.5
- mlp_gain: float32 [2048], replicated, may hold values from 0.1 to 1.9
- w_up: bfloat16 [2048, 8192], P('kv', 'tp'), may hold values from -0.125 to 0.125
- w_down: bfloat16 [8192, 2048], P('tp', 'kv'), may hold values from -0.0625 to 0.0625
Outputs:
- next_resid: bfloat16 [12, 2048], P(('grp', 'dp'), ('kv', 'tp')), parts along dimension 0
There are 2 independent parts, one for each index of `grp`. A program takes and returns all parts, laid end to end along the dimension named above; an argument that names none is the same for every part. Nothing has to cross between parts.
Inputs may be any that keep to these rules, and one draw needn't show every extreme that they name: gates_cache[b, p, g] is the sum of the log forget gates of the cached positions after p, so it never falls along the positions and is 0 at the last one.
All inputs are finite; a program needn't handle non-finite values.
Results may differ from a plain program's by a relative error of at most 0.028.
Values may be sent and summed in bfloat16 or wider, within the bound.
A program may use at most 64 MiB of HBM per device.

v0:
```python
import jax
import jax.numpy as jnp
from jax import lax
from jax.sharding import PartitionSpec as P

D = 2048
HEADS = 32
LOOKUP_GROUPS = 4
HEAD = 64


EPS = 1e-06


def joined(value, axis, join):
    pieces = jax.tree.map(lambda part: lax.all_gather(part, axis), value)
    head = jax.tree.map(lambda part: part[0], pieces)
    tail = jax.tree.map(lambda part: part[1:], pieces)
    running, _ = lax.scan(lambda running, section: (join(running, section), None), head, tail)
    return running


def prepare_rows(source, gain_vector, offset, width_block):
    own_block = lax.all_gather(source, "tp", axis=1, tiled=True).astype(jnp.float32)
    squares = jnp.sum(own_block * own_block, axis=1, keepdims=True)
    gain_block = lax.dynamic_slice_in_dim(gain_vector, offset, width_block, 0)
    scaled = (own_block * gain_block).astype(jnp.bfloat16)
    return (scaled, squares, None)


def merge_parts(earlier, later):
    peak_a, total_a, mixed_a = earlier
    peak_b, total_b, mixed_b = later
    new_peak = jnp.maximum(peak_a, peak_b)
    scale_a = jnp.exp(peak_a - new_peak)
    scale_b = jnp.exp(peak_b - new_peak)
    return (
        new_peak,
        total_a * scale_a + total_b * scale_b,
        mixed_a * scale_a[..., None] + mixed_b * scale_b[..., None],
    )


def shards(
    resid,
    keys_cache,
    values_cache,
    gates_cache,
    norm_gain,
    w_query,
    w_key,
    w_value,
    w_forget,
    forget_bias,
    w_out,
    mlp_gain,
    w_up,
    w_down,
):
    row_count = resid.shape[0]
    width_block = w_query.shape[0]
    offset = lax.axis_index("kv") * width_block
    local_heads = w_key.shape[1] // HEAD
    group_size = HEADS // LOOKUP_GROUPS
    head_offset = lax.axis_index("tp") * local_heads
    scaled, squares, inverse = prepare_rows(resid, norm_gain, offset, width_block)
    forget_rows = lax.dynamic_slice(w_forget, (offset, head_offset), (width_block, local_heads))
    query_part = jnp.dot(scaled, w_query, preferred_element_type=jnp.float32)
    key_part = jnp.dot(scaled, w_key, preferred_element_type=jnp.float32)
    value_part = jnp.dot(scaled, w_value, preferred_element_type=jnp.float32)
    forget_part = jnp.dot(scaled, forget_rows, preferred_element_type=jnp.float32)
    query_sum, key_sum, value_sum, forget_sum, norm_total = lax.psum(
        (query_part, key_part, value_part, forget_part, squares), "kv"
    )
    inverse = lax.rsqrt(norm_total / D + EPS)
    bias_local = lax.dynamic_slice_in_dim(forget_bias, head_offset, local_heads, 0)
    log_forget = jax.nn.log_sigmoid(forget_sum * inverse + bias_local)
    query = (
        (query_sum * inverse).astype(jnp.bfloat16).reshape(row_count, local_heads, group_size, HEAD)
    )
    key_new = (key_sum * inverse).astype(jnp.bfloat16).reshape(row_count, local_heads, HEAD)
    value_new = (value_sum * inverse).astype(jnp.bfloat16).reshape(row_count, local_heads, HEAD)
    ctx_len = keys_cache.shape[1]
    cached_keys = keys_cache.reshape(row_count, ctx_len, local_heads, HEAD)
    cached_values = values_cache.reshape(row_count, ctx_len, local_heads, HEAD)
    score_scale = HEAD ** (-0.5)
    scores = (
        jnp.einsum("bgjd,bpgd->bgjp", query, cached_keys, preferred_element_type=jnp.float32)
        * score_scale
    )
    gate_bias = jnp.transpose(gates_cache, (0, 2, 1)) + log_forget[:, :, None]
    scores = scores + gate_bias[:, :, None, :]
    maxima = jnp.max(scores, axis=3)
    weights = jnp.exp(scores - maxima[..., None])
    totals = jnp.sum(weights, axis=3)
    mixed = jnp.einsum(
        "bgjp,bpgd->bgjd",
        weights.astype(jnp.bfloat16),
        cached_values,
        preferred_element_type=jnp.float32,
    )
    maxima, totals, mixed = joined((maxima, totals, mixed), "kv", merge_parts)
    fresh = (
        jnp.einsum("bgjd,bgd->bgj", query, key_new, preferred_element_type=jnp.float32)
        * score_scale
    )
    new_peak = jnp.maximum(maxima, fresh)
    carried = jnp.exp(maxima - new_peak)
    own_weight = jnp.exp(fresh - new_peak)
    totals = totals * carried + own_weight
    mixed = mixed * carried[..., None] + jnp.einsum(
        "bgj,bgd->bgjd",
        own_weight.astype(jnp.bfloat16),
        value_new,
        preferred_element_type=jnp.float32,
    )
    attended = (
        (mixed / totals[..., None])
        .astype(jnp.bfloat16)
        .reshape(row_count, local_heads * group_size * HEAD)
    )
    out_part = jnp.dot(attended, w_out, preferred_element_type=jnp.float32)
    branch = lax.psum_scatter(
        out_part.astype(jnp.bfloat16), "tp", scatter_dimension=1, tiled=True
    ).astype(jnp.float32)
    middle = (resid.astype(jnp.float32) + branch).astype(jnp.bfloat16)
    scaled_mid, squares_mid, inverse_mid = prepare_rows(middle, mlp_gain, offset, width_block)
    up_part = jnp.dot(scaled_mid, w_up, preferred_element_type=jnp.float32)
    up_total, norm_mid = (
        lax.psum(up_part.astype(jnp.bfloat16), "kv").astype(jnp.float32),
        lax.psum(squares_mid.astype(jnp.bfloat16), "kv").astype(jnp.float32),
    )
    inverse_mid = lax.rsqrt(norm_mid / D + EPS)
    hidden = jnp.square(jax.nn.relu(up_total * inverse_mid)).astype(jnp.bfloat16)
    down_part = jnp.dot(hidden, w_down, preferred_element_type=jnp.float32)
    mixer_out = lax.psum_scatter(
        down_part.astype(jnp.bfloat16), "tp", scatter_dimension=1, tiled=True
    ).astype(jnp.float32)
    return (middle.astype(jnp.float32) + mixer_out).astype(jnp.bfloat16)


def solution(mesh):
    in_specs = (
        P(("grp", "dp"), ("kv", "tp")),
        P(("grp", "dp"), "kv", "tp"),
        P(("grp", "dp"), "kv", "tp"),
        P(("grp", "dp"), "kv", "tp"),
        P(),
        P("kv", "tp"),
        P("kv", "tp"),
        P("kv", "tp"),
        P(),
        P(),
        P("tp", "kv"),
        P(),
        P("kv", "tp"),
        P("tp", "kv"),
    )
    out_specs = P(("grp", "dp"), ("kv", "tp"))
    return jax.shard_map(shards, mesh=mesh, in_specs=in_specs, out_specs=out_specs, check_vma=False)
```

profile of v0, /device:TPU:0, one launch (start us, length us, event | category | flops | bytes accessed | tf_op | source)
XLA Modules:
  0.0 130.3 jit_solution(91823296636983148)
XLA Ops:
  6.5 2.2 %all_gather.24 = bf16[3,512]{1,0:T(4,128)(2,1)S(1)} all-gather(bf16[3,256]{1,0:T(4,128)(2,1)} %param.16), channel_id=1, replica_groups=mesh['grp'=2,'dp'=2,'kv'=4,'tp'=2] {'tp'}, dimensions={1}, use_global_device_ids=true | all-gather | bytes 4608 | tf_op jit(solution)/shard_map/all_gather | solution.py:24
  8.8 0.8 dynamic_slice.23
  9.9 1.0 fusion.28
  11.0 1.1 fusion.30
  12.0 0.9 fusion.19
  12.9 20.5 %all-reduce = (f32[3,1024]{1,0:T(4,128)S(1)}, f32[3,1]{0,1:T(1,128)S(1)}, f32[3,2]{0,1:T(2,128)S(1)}, f32[3,128]{1,0:T(4,128)S(1)}, f32[3,128]{1,0:T(4,128)S(1)}) all-reduce(f32[3,1024]{1,0:T(4,128)S(1)} %fusion.27, f32[3,1]{0,1:T(1,128)S(1)} %bitcast.69, ...), channel_id=1, replica_groups=mesh['grp'=2,'dp'=2,'kv'=4,'tp'=2] {'kv'}, use_global_device_ids=true, to_apply=%region_0.0 | all-reduce | flops 3849 | bytes 30792 | tf_op jit(solution)/shard_map/psum | solution.py:72
  33.6 0.7 dynamic_slice.25
  34.5 1.4 %copy.21 = bf16[3,1024,128]{1,2,0:T(8,128)(2,1)S(1)} copy(bf16[3,1024,128]{2,1,0:T(8,128)(2,1)} %param.17) | data formatting | bytes 1572864 | tf_op args[1]
  35.9 1.4 %copy.23 = bf16[3,1024,128]{1,2,0:T(8,128)(2,1)S(1)} copy(bf16[3,1024,128]{2,1,0:T(8,128)(2,1)} %param.18) | data formatting | bytes 1572864 | tf_op args[2]
  38.1 13.2 %all-gather.2 = f32[12,2,8,64]{3,2,1,0:T(8,128)S(1)} all-gather(f32[3,2,8,64]{3,2,1,0:T(8,128)S(1)} %fusion.6), channel_id=4, replica_groups=mesh['grp'=2,'dp'=2,'kv'=4,'tp'=2] {'kv'}, dimensions={0}, use_global_device_ids=true | all-gather | bytes 61440 | tf_op jit(solution)/shard_map/all_gather | solution.py:16
  51.6 13.1 %all-gather.1 = f32[12,2,8]{2,1,0:T(2,128)S(1)} all-gather(f32[3,2,8]{2,1,0:T(2,128)S(1)} %fusion.5), channel_id=3, replica_groups=mesh['grp'=2,'dp'=2,'kv'=4,'tp'=2] {'kv'}, dimensions={0}, use_global_device_ids=true | all-gather | bytes 960 | tf_op jit(solution)/shard_map/all_gather | solution.py:16
  64.7 13.1 %all-gather = f32[12,2,8]{2,1,0:T(2,128)S(1)} all-gather(f32[3,2,8]{2,1,0:T(2,128)S(1)} %get-tuple-element.79), channel_id=2, replica_groups=mesh['grp'=2,'dp'=2,'kv'=4,'tp'=2] {'kv'}, dimensions={0}, use_global_device_ids=true | all-gather | bytes 960 | tf_op jit(solution)/shard_map/all_gather | solution.py:16
  78.8 1.5 %convolution_convert_fusion.2 = bf16[3,512]{1,0:T(4,128)(2,1)S(1)} fusion(bf16[3,1024]{1,0:T(4,128)(2,1)S(1)} %reshape.44, bf16[1024,512]{1,0:T(8,128)(2,1)} %param.26), kind=kOutput, calls=%fused_computation.12 | convolution fusion | flops 3147264 | bytes 1057792 | tf_op jit(solution)/shard_map/dot_general | solution.py:122
  80.3 0.8 copy.26
  81.1 0.8 dynamic_slice.26
  81.9 5.1 %reduce-scatter.7.cloned.1.call-done = bf16[256,3]{1,0:T(8,128)(2,1)} async-done(((bf16[512,3]{1,0:T(8,128)(2,1)}), bf16[256,3]{1,0:T(8,128)(2,1)}) %reduce-scatter.7.cloned.1.call-update) | async-done | bytes 1552
  87.1 0.9 copy.27
  88.0 1.8 %all_gather.31 = bf16[3,512]{1,0:T(4,128)(2,1)S(1)} all-gather(bf16[3,256]{1,0:T(4,128)(2,1)S(1)} %add_convert_fusion.1), channel_id=1, replica_groups=mesh['grp'=2,'dp'=2,'kv'=4,'tp'=2] {'tp'}, dimensions={1}, use_global_device_ids=true | all-gather | bytes 4608 | tf_op jit(solution)/shard_map/all_gather | solution.py:24
  90.0 2.8 %convolution_convert_fusion = bf16[3,4096]{1,0:T(4,128)(2,1)S(1)} fusion(bf16[512,4096]{1,0:T(8,128)(2,1)} %param.28, bf16[3,512]{1,0:T(4,128)(2,1)S(1)} %all_gather.31, f32[512]{0:T(512)S(1)} %dynamic_slice.26), kind=kOutput, calls=%fused_computation.8 | convolution fusion | flops 12599808 | bytes 4224000 | tf_op jit(solution)/shard_map/dot_general | solution.py:128
  92.8 19.5 %all-reduce.1 = (bf16[3,4096]{1,0:T(4,128)(2,1)S(1)}, bf16[3,1]{0,1:T(2,128)(2,1)S(1)}) all-reduce(bf16[3,4096]{1,0:T(4,128)(2,1)S(1)} %convolution_convert_fusion, bf16[3,1]{0,1:T(2,128)(2,1)S(1)} %bitcast.68), channel_id=1, replica_groups=mesh['grp'=2,'dp'=2,'kv'=4,'tp'=2] {'kv'}, use_global_device_ids=true, to_apply=%region_11.12 | all-reduce | flops 12291 | bytes 49164 | tf_op jit(solution)/shard_map/psum | solution.py:130
  112.4 2.9 %convolution_convert_fusion.1 = bf16[3,512]{1,0:T(4,128)(2,1)S(1)} fusion(bf16[4096,512]{1,0:T(8,128)(2,1)} %param.29, bf16[3,4096]{1,0:T(4,128)(2,1)S(1)} %get-tuple-element.66, f32[3]{0:T(128)S(1)} %rsqrt_bitcast_fusion), kind=kOutput, calls=%fused_computation.11 | convolution fusion | flops 12645888 | bytes 4221964 | tf_op jit(solution)/shard_map/dot_general | solution.py:135
  115.2 0.8 copy.28
  116.1 5.9 %reduce-scatter.9.cloned.1.call-done = bf16[256,3]{1,0:T(8,128)(2,1)} async-done(((bf16[512,3]{1,0:T(8,128)(2,1)}), bf16[256,3]{1,0:T(8,128)(2,1)}) %reduce-scatter.9.cloned.1.call-update) | async-done | bytes 1552
  122.0 0.9 copy.29
  (45 shorter events, 3.8 us)
Async XLA Ops:
  6.5 3.1 %copy-start = (bf16[512,1024]{1,0:T(8,128)(2,1)S(1)}, bf16[512,1024]{1,0:T(8,128)(2,1)}, u32[]{:S(2)}) copy-start(bf16[512,1024]{1,0:T(8,128)(2,1)} %param.21) | copy-start | bytes 3145732
  6.5 30.8 %copy-start.1 = (f32[3,1024,2]{1,2,0:T(2,128)S(1)}, f32[3,1024,2]{1,2,0:T(2,128)}, u32[]{:S(2)}) copy-start(f32[3,1024,2]{1,2,0:T(2,128)} %param.19) | copy-start | bytes 73732
  6.5 80.5 %reduce-scatter.7.cloned.1.call-start = ((), (), s32[]{:S(2)}) async-start(), calls=%async_computation.2 | async-start | bytes 196608
  11.0 77.0 %copy-start.2 = (bf16[3,256]{1,0:T(4,128)(2,1)S(1)}, bf16[3,256]{1,0:T(4,128)(2,1)}, u32[]{:S(2)}) copy-start(bf16[3,256]{1,0:T(4,128)(2,1)} %param.16) | copy-start | bytes 4612
  81.1 40.9 %reduce-scatter.9.cloned.1.call-start = ((), (), s32[]{:S(2)}) async-start(), calls=%async_computation.3 | async-start | bytes 196608
Sparse Core Ops, SparseCore 0:
  81.2 5.7 reduce-scatter.6
  116.2 5.7 reduce-scatter.8
where the time goes:
time: 131 us; the launch traced here: 130 us
  blocking collectives  83.7 us (64%)
  between operations  13.5 us (10%)
  matrix products  11.2 us (9%)
  waiting for transfers between devices  11.1 us (8%)
  local copies, waits for them, and re-layouts  8.98 us (7%)
  other arithmetic  1.82 us (1%)
    all_gather x3, blocking collectives, joined(): pieces = jax.tree.map(lambda part: lax.all_gather(part, axis), value)  39.5 us
    psum x1, blocking collectives, shards(): lax.psum((query_part, key_part, value_part, forget_part, squares), 'kv')  20.5 us
    psum x1, blocking collectives, shards(): lax.psum(up_part.astype(jnp.bfloat16), 'kv').astype(jnp.float32)  19.5 us
    unnamed x4, waiting for transfers between devices  11.1 us
    unnamed x12, local copies, waits for them, and re-layouts  6.26 us
    all_gather x2, blocking collectives, prepare_rows(): lax.all_gather(source, 'tp', axis=1, tiled=True).astype(jnp.float32)  4.08 us
    dot_general x1, matrix products, shards(): down_part = jnp.dot(hidden, w_down, preferred_element_type=jnp.float32)  2.87 us
    dot_general x1, matrix products, shards(): up_part = jnp.dot(scaled_mid, w_up, preferred_element_type=jnp.float32)  2.84 us
  transfers between devices with their start and end apart: 2, of which 2 were waited for; matrix products, arithmetic and copies ran while one was open for 1% of the time, Pallas kernels for 0%

commit v1 on v0

v1 whole, which is shorter than its diff:
```python
import functools

import jax
import jax.numpy as jnp
from jax import lax
from jax.experimental import pallas as pl
from jax.experimental.pallas import tpu as pltpu
from jax.sharding import PartitionSpec as P

HEADS = 32
LOOKUP_GROUPS = 4
HEAD = 64
EPS = 1e-06
CHUNKS = 4
MESH = pl.DeviceIdType.MESH
F32 = jnp.float32
BF16 = jnp.bfloat16


def layer_kernel(
    n_kv,
    n_tp,
    resid,
    keys,
    values,
    gates,
    gain1,
    w_query,
    w_key,
    w_value,
    w_forget_t,
    bias,
    w_out,
    gain2,
    w_up,
    w_down,
    out,
    halves,
    gain1_v,
    wqkv,
    wf_v,
    bias_v,
    keys_v,
    values_v,
    gates_v,
    wo_v,
    gain2_v,
    wu_v,
    wd_v,
    proj,
    qs,
    soft,
    att,
    branch,
    norm2,
    ups,
    tail_out,
    tail_in,
    load_sem,
    tp_send,
    tp_recv,
    kv_send,
    kv_recv,
):
    kv = lax.axis_index("kv")
    tp = lax.axis_index("tp")
    peer = lax.rem(tp + 1, n_tp)
    rows, half = resid.shape
    width = half * n_tp
    features = width * n_kv
    qw = w_query.shape[1]
    kw = w_key.shape[1]
    local_heads = kw // HEAD
    group = HEADS // LOOKUP_GROUPS
    ff = w_up.shape[1]
    ff_chunk = ff // CHUNKS

    def load(index, source, target):
        copy = pltpu.make_async_copy(source, target, load_sem.at[index])
        copy.start()
        return copy

    load_resid = load(0, resid, halves.at[tp])
    load_gain1 = load(1, gain1, gain1_v)
    load_wq = load(2, w_query, wqkv.at[:, pl.ds(0, qw)])
    load_wk = load(3, w_key, wqkv.at[:, pl.ds(qw, kw)])
    load_wv = load(4, w_value, wqkv.at[:, pl.ds(qw + kw, kw)])
    load_wf = load(5, w_forget_t, wf_v)
    load_bias = load(6, bias, bias_v)

    barrier = pltpu.get_barrier_semaphore()
    pl.semaphore_signal(barrier, inc=1, device_id={"tp": peer}, device_id_type=MESH)
    for step in range(1, n_kv):
        pl.semaphore_signal(
            barrier, inc=1, device_id={"kv": lax.rem(kv + step, n_kv)}, device_id_type=MESH
        )
    load_keys = load(7, keys, keys_v)
    load_gates = load(8, gates, gates_v)
    load_values = load(9, values, values_v)
    load_wo = load(10, w_out, wo_v)
    load_gain2 = load(11, gain2, gain2_v)
    load_wu = load(12, w_up, wu_v)
    load_wd = load(13, w_down, wd_v)
    sends = []

    def to_peer(index, source, target):
        copy = pltpu.make_async_remote_copy(
            src_ref=source,
            dst_ref=target,
            send_sem=tp_send.at[index],
            recv_sem=tp_recv.at[index],
            device_id={"tp": peer},
            device_id_type=MESH,
        )
        copy.start()
        sends.append(copy)
        return copy

    def to_all(index, block):
        copies = []
        for step in range(1, n_kv):
            slot = index * (n_kv - 1) + step - 1
            copy = pltpu.make_async_remote_copy(
                src_ref=block,
                dst_ref=block,
                send_sem=kv_send.at[slot],
                recv_sem=kv_recv.at[slot],
                device_id={"kv": lax.rem(kv + step, n_kv)},
                device_id_type=MESH,
            )
            copy.start()
            copies.append(copy)
        sends.extend(copies)
        return copies

    load_resid.wait()
    pl.semaphore_wait(barrier, n_kv)
    swap = to_peer(0, halves.at[tp], halves.at[tp])
    load_gain1.wait()
    load_wq.wait()
    load_wk.wait()
    load_wv.wait()
    load_wf.wait()
    load_bias.wait()
    swap.wait_recv()

    offset = pl.multiple_of(kv * width, 128)
    lane = lax.broadcasted_iota(jnp.int32, (1, 128), 1)
    source = jnp.concatenate([halves[i].astype(F32) for i in range(n_tp)], axis=1)
    scaled = (source * gain1_v[:, pl.ds(offset, width)]).astype(BF16)
    squares = jnp.sum(source * source, axis=1, keepdims=True)
    proj[kv, :rows, : qw + 2 * kw] = jnp.dot(scaled, wqkv[...], preferred_element_type=F32)
    wf = wf_v[:, pl.ds(offset, width)].astype(F32)
    scaled32 = scaled.astype(F32)
    extra = jnp.broadcast_to(squares, (rows, 128))
    bias_rows = []
    for h in range(local_heads):
        picked = wf[h : h + 1]
        bias_h = bias_v[:, h : h + 1]
        for t in range(1, n_tp):
            g = t * local_heads + h
            picked = jnp.where(tp == t, wf[g : g + 1], picked)
            bias_h = jnp.where(tp == t, bias_v[:, g : g + 1], bias_h)
        bias_rows.append(bias_h)
        gate = jnp.sum(scaled32 * picked, axis=1, keepdims=True)
        extra = jnp.where(lane == h, gate, extra)
    proj[kv, :rows, qw + 2 * kw :] = extra

    copies = to_all(0, proj.at[kv])
    load_keys.wait()
    load_gates.wait()
    load_values.wait()
    for copy in copies:
        copy.wait_recv()
    total = proj[0, :rows, :]
    for i in range(1, n_kv):
        total = total + proj[i, :rows, :]
    extra = total[:, qw + 2 * kw :]
    inverse = lax.rsqrt(extra[:, local_heads : local_heads + 1] / features + EPS)
    query = (total[:, :qw] * inverse).astype(BF16).astype(F32) * (HEAD ** (-0.5))
    key_new = (total[:, qw : qw + kw] * inverse).astype(BF16).astype(F32)
    value_new = (total[:, qw + kw : qw + 2 * kw] * inverse).astype(BF16).astype(F32)
    low = lane < HEAD
    per_row = local_heads * group
    for t in range(group // 2):
        for h in range(local_heads):
            start = h * group * HEAD + t * 128
            block = query[:, start : start + 128]
            turned = pltpu.roll(block, HEAD, 1)
            first, second = (block, turned) if h == 0 else (turned, block)
            keep = low if h == 0 else jnp.logical_not(low)
            for j, item in ((2 * t, first), (2 * t + 1, second)):
                kept = jnp.where(keep, item, 0.0)
                for b in range(rows):
                    row = b * per_row + h * group + j
                    qs[row : row + 1, :] = kept[b : b + 1, :]
    forget = []
    for h in range(local_heads):
        z = extra[:, h : h + 1] * inverse + bias_rows[h]
        forget.append(jnp.minimum(z, 0.0) - jnp.log1p(jnp.exp(-jnp.abs(z))))

    def both(pair):
        return jnp.where(low, pair[:group], pair[group:])

    front = jnp.bitwise_and(lane, HEAD - 1) < HEAD // 2
    for b in range(rows):
        q_b = qs[b * per_row : (b + 1) * per_row, :].astype(BF16)
        scores = lax.dot_general(
            q_b, keys_v[b], (((1,), (1,)), ((), ())), preferred_element_type=F32
        )
        ctx = scores.shape[1]
        scores = scores + jnp.concatenate(
            [
                jnp.broadcast_to(gates_v[b, h : h + 1, :], (group, ctx))
                for h in range(local_heads)
            ],
            axis=0,
        )
        maxima = jnp.max(scores, axis=1, keepdims=True)
        weights = jnp.exp(scores - maxima)
        totals = jnp.sum(weights, axis=1, keepdims=True)
        mixed = jnp.dot(weights.astype(BF16), values_v[b], preferred_element_type=F32)
        peak = both(maxima) + jnp.where(low, forget[0][b : b + 1], forget[1][b : b + 1])
        soft[kv, 0, b * group : (b + 1) * group, :] = both(mixed)
        soft[kv, 1, b * group : (b + 1) * group, :] = jnp.where(front, peak, both(totals))
    copies = to_all(1, soft.at[kv])
    fresh, fresh_value = [], []
    for b in range(rows):
        q_b = qs[b * per_row : (b + 1) * per_row, :]
        fresh.append(both(jnp.sum(q_b * key_new[b : b + 1], axis=1, keepdims=True)))
        fresh_value.append(jnp.broadcast_to(value_new[b : b + 1], (group, 128)))
    fresh = jnp.concatenate(fresh, axis=0)
    fresh_value = jnp.concatenate(fresh_value, axis=0)
    for copy in copies:
        copy.wait_recv()
    peaks, counts = [], []
    for i in range(n_kv):
        stat = soft[i, 1]
        peaks.append(jnp.where(front, stat, pltpu.roll(stat, HEAD // 2, 1)))
        counts.append(jnp.where(front, pltpu.roll(stat, 128 - HEAD // 2, 1), stat))
    peak = fresh
    for item in peaks:
        peak = jnp.maximum(peak, item)
    own = jnp.exp(fresh - peak)
    count = own
    mixed = own.astype(BF16).astype(F32) * fresh_value
    for i in range(n_kv):
        scale = jnp.exp(peaks[i] - peak)
        count = count + counts[i] * scale
        mixed = mixed + soft[i, 0] * scale
    att[...] = mixed / count
    blocks = [[] for _ in range(local_heads)]
    for t in range(group // 2):
        pair = []
        for j in (2 * t, 2 * t + 1):
            pair.append(
                jnp.concatenate(
                    [att[b * group + j : b * group + j + 1, :] for b in range(rows)], axis=0
                )
            )
        blocks[0].append(jnp.where(low, pair[0], pltpu.roll(pair[1], HEAD, 1)))
        blocks[1].append(jnp.where(low, pltpu.roll(pair[0], HEAD, 1), pair[1]))
    attended = jnp.concatenate(blocks[0] + blocks[1], axis=1).astype(BF16)

    load_wo.wait()
    branch[tp, :rows, :] = jnp.dot(attended, wo_v[...], preferred_element_type=F32).astype(BF16)
    swap = to_peer(1, branch.at[tp], branch.at[tp])
    load_gain2.wait()
    load_wu.wait()
    swap.wait_recv()
    added = branch[0, :rows, :].astype(F32)
    for t in range(1, n_tp):
        added = added + branch[t, :rows, :].astype(F32)
    middle = (source + added).astype(BF16).astype(F32)
    scaled = (middle * gain2_v[:, pl.ds(offset, width)]).astype(BF16)
    squares = jnp.sum(middle * middle, axis=1, keepdims=True)
    norm2[kv, :rows, :] = jnp.broadcast_to(squares, (rows, 128))
    norm_copies = to_all(2, norm2.at[kv])
    up_copies = []
    for c in range(CHUNKS):
        ups[c, kv, :rows, :] = jnp.dot(
            scaled, wu_v[:, c * ff_chunk : (c + 1) * ff_chunk], preferred_element_type=F32
        ).astype(BF16)
        up_copies.append(to_all(3 + c, ups.at[c, kv]))
    load_wd.wait()
    for copy in norm_copies:
        copy.wait_recv()
    squares = norm2[0, :rows, :1]
    for i in range(1, n_kv):
        squares = squares + norm2[i, :rows, :1]
    inverse = lax.rsqrt(squares / features + EPS)
    down = jnp.zeros((rows, width), F32)
    for c in range(CHUNKS):
        for copy in up_copies[c]:
            copy.wait_recv()
        up = ups[c, 0, :rows, :].astype(F32)
        for i in range(1, n_kv):
            up = up + ups[c, i, :rows, :].astype(F32)
        hidden = jnp.square(jnp.maximum(up * inverse, 0.0)).astype(BF16)
        down = down + jnp.dot(
            hidden, wd_v[c * ff_chunk : (c + 1) * ff_chunk, :], preferred_element_type=F32
        )

    def part(value, which):
        picked = value[:, :half]
        for t in range(1, n_tp):
            picked = jnp.where(which == t, value[:, t * half : (t + 1) * half], picked)
        return picked

    tail_out[:rows, :] = part(down, peer).astype(BF16)
    swap = to_peer(2, tail_out, tail_in)
    kept = part(down, tp).astype(BF16).astype(F32)
    middle_half = part(middle, tp)
    swap.wait_recv()
    out[...] = (middle_half + (kept + tail_in[:rows, :].astype(F32))).astype(BF16)
    for copy in sends:
        copy.wait_send()


def layer(
    n_kv,
    n_tp,
    resid,
    keys_cache,
    values_cache,
    gates_cache,
    norm_gain,
    w_query,
    w_key,
    w_value,
    w_forget,
    forget_bias,
    w_out,
    mlp_gain,
    w_up,
    w_down,
):
    rows, half = resid.shape
    padded = -(-rows // 4) * 4
    width = half * n_tp
    qw, kw, ff = w_query.shape[1], w_key.shape[1], w_up.shape[1]
    group = HEADS // LOOKUP_GROUPS
    local_heads = kw // HEAD
    gates = jnp.transpose(gates_cache, (0, 2, 1))
    gain1, gain2 = norm_gain.reshape(1, -1), mlp_gain.reshape(1, -1)
    forget_t = jnp.transpose(w_forget)
    bias = forget_bias.reshape(1, -1)
    exchanges = 3 + CHUNKS
    return pl.pallas_call(
        functools.partial(layer_kernel, n_kv, n_tp),
        out_shape=jax.ShapeDtypeStruct((rows, half), BF16),
        in_specs=[pl.BlockSpec(memory_space=pl.ANY)] * 14,
        out_specs=pl.BlockSpec(memory_space=pltpu.VMEM),
        scratch_shapes=[
            pltpu.VMEM((n_tp, rows, half), BF16),
            pltpu.VMEM(gain1.shape, F32),
            pltpu.VMEM((w_query.shape[0], qw + 2 * kw), BF16),
            pltpu.VMEM(forget_t.shape, BF16),
            pltpu.VMEM(bias.shape, F32),
            pltpu.VMEM(keys_cache.shape, BF16),
            pltpu.VMEM(values_cache.shape, BF16),
            pltpu.VMEM(gates.shape, F32),
            pltpu.VMEM(w_out.shape, BF16),
            pltpu.VMEM(gain2.shape, F32),
            pltpu.VMEM(w_up.shape, BF16),
            pltpu.VMEM(w_down.shape, BF16),
            pltpu.VMEM((n_kv, padded, qw + 2 * kw + 128), F32),
            pltpu.VMEM((rows * local_heads * group, 128), F32),
            pltpu.VMEM((n_kv, 2, rows * group, 128), F32),
            pltpu.VMEM((rows * group, 128), F32),
            pltpu.VMEM((n_tp, padded, width), BF16),
            pltpu.VMEM((n_kv, padded, 128), F32),
            pltpu.VMEM((CHUNKS, n_kv, padded, ff // CHUNKS), BF16),
            pltpu.VMEM((padded, half), BF16),
            pltpu.VMEM((padded, half), BF16),
            pltpu.SemaphoreType.DMA((14,)),
            pltpu.SemaphoreType.DMA((3,)),
            pltpu.SemaphoreType.DMA((3,)),
            pltpu.SemaphoreType.DMA((exchanges * (n_kv - 1),)),
            pltpu.SemaphoreType.DMA((exchanges * (n_kv - 1),)),
        ],
        compiler_params=pltpu.CompilerParams(
            collective_id=0, has_side_effects=True, vmem_limit_bytes=60 * 1024 * 1024
        ),
    )(
        resid,
        keys_cache,
        values_cache,
        gates,
        gain1,
        w_query,
        w_key,
        w_value,
        forget_t,
        bias,
        w_out,
        gain2,
        w_up,
        w_down,
    )


def solution(mesh):
    in_specs = (
        P(("grp", "dp"), ("kv", "tp")),
        P(("grp", "dp"), "kv", "tp"),
        P(("grp", "dp"), "kv", "tp"),
        P(("grp", "dp"), "kv", "tp"),
        P(),
        P("kv", "tp"),
        P("kv", "tp"),
        P("kv", "tp"),
        P(),
        P(),
        P("tp", "kv"),
        P(),
        P("kv", "tp"),
        P("tp", "kv"),
    )
    body = functools.partial(layer, mesh.shape["kv"], mesh.shape["tp"])
    return jax.shard_map(
        body,
        mesh=mesh,
        in_specs=in_specs,
        out_specs=P(("grp", "dp"), ("kv", "tp")),
        check_vma=False,
    )
```

time: 131 us -> 25.1 us (0.19)
  blocking collectives: 83.7 us -> 0 us
  Pallas kernels: 0 us -> 23.6 us
  between operations: 13.5 us -> 0.01 us
  matrix products: 11.2 us -> 0 us
  waiting for transfers between devices: 11.1 us -> 0 us
  local copies, waits for them, and re-layouts: 8.98 us -> 1.26 us
  other arithmetic: 1.82 us -> 0 us
    all_gather x5 -> x0, blocking collectives: 43.6 us -> none  [the longest x3 39.5 us: joined(): pieces = jax.tree.map(lambda part: lax.all_gather(part, axis), value)]
    psum x2 -> x0, blocking collectives: 40.1 us -> none  [the longest x1 20.5 us: shards(): lax.psum((query_part, key_part, value_part, forget_part, squares), 'kv')]
    pallas_call x0 -> x1, Pallas kernels: none -> 23.6 us  [layer(): pl.pallas_call(functools.partial(layer_kernel, n_kv, n_tp), out_shape=jax...]
    dot_general x10 -> x0, matrix products: 11.2 us -> none  [the longest x1 2.87 us: shards(): down_part = jnp.dot(hidden, w_down, preferred_element_type=jnp.float32)]
    unnamed x4 -> x0, waiting for transfers between devices: 11.1 us -> none
    unnamed x12 -> x1, local copies, waits for them, and re-layouts: 6.26 us -> 1.26 us
    dynamic_slice x3 -> x0, local copies, waits for them, and re-layouts: 2.26 us -> none  [the longest x2 1.53 us: prepare_rows(): gain_block = lax.dynamic_slice_in_dim(gain_vector, offset, width_block, 0)]
  transfers between devices with their start and end apart: 2 -> 0, of which waited for: 2 -> 0; matrix products, arithmetic and copies ran while one was open for 1% -> 0% of each run, Pallas kernels for 0% -> 0%
where the time goes in v1:
time: 25.1 us; the launch traced here: 24.9 us
  Pallas kernels  23.6 us (94%)
  local copies, waits for them, and re-layouts  1.26 us (5%)
    pallas_call x1, Pallas kernels, layer(): pl.pallas_call(functools.partial(layer_kernel, n_kv, n_tp), out_shape=jax...  23.6 us
    unnamed x1, local copies, waits for them, and re-layouts  1.26 us

profile of v1, /device:TPU:0, one launch (start us, length us, event | category | flops | bytes accessed | tf_op | source)
XLA Modules:
  0.0 24.9 jit_solution(12742672377752708624)
XLA Ops:
  0.0 23.6 %shard_map.136 = bf16[3,256]{1,0:T(4,128)(2,1)} custom-call(bf16[3,256]{1,0:T(4,128)(2,1)} %resid.1, bf16[3,1024,128]{2,1,0:T(8,128)(2,1)} %keys.1, bf16[3,1024,128]{2,1,0:T(8,128)(2,1)} %values.1, f32[3,2,1024]{2,1,0:T(2,128)} %bitcast.5, f32[1,2048]{1,0:T(1,128)} %bitcast.7, bf16[512,1024]{1,0:T(8,128)(2,1)} %w_query.1, bf16[512,128]{1,0:T(8,128)(2,1)} %w_key.1, ...), custom_call_target="tpu_custom_call" | custom-call | tf_op jit(solution)/shard_map/pallas_call | solution.py:349
  23.6 1.3 %copy.16 = bf16[3,256]{1,0:T(4,128)(2,1)} copy(bf16[3,256]{1,0:T(4,128)(2,1)} %shard_map.136) | data formatting | bytes 3072

commit v2 on v1

--- a/solution.py
+++ b/solution.py
@@ -136,24 +136,22 @@
     load_resid.wait()
     pl.semaphore_wait(barrier, n_kv)
     swap = to_peer(0, halves.at[tp], halves.at[tp])
+    lane = lax.broadcasted_iota(jnp.int32, (1, 128), 1)
+    slot = jnp.bitwise_and(lane, HEAD - 1)
+
+    def part(value, which):
+        picked = value[:, :half]
+        for t in range(1, n_tp):
+            picked = jnp.where(which == t, value[:, t * half : (t + 1) * half], picked)
+        return picked
+
     load_gain1.wait()
-    load_wq.wait()
-    load_wk.wait()
-    load_wv.wait()
     load_wf.wait()
     load_bias.wait()
-    swap.wait_recv()
-
     offset = pl.multiple_of(kv * width, 128)
-    lane = lax.broadcasted_iota(jnp.int32, (1, 128), 1)
-    source = jnp.concatenate([halves[i].astype(F32) for i in range(n_tp)], axis=1)
-    scaled = (source * gain1_v[:, pl.ds(offset, width)]).astype(BF16)
-    squares = jnp.sum(source * source, axis=1, keepdims=True)
-    proj[kv, :rows, : qw + 2 * kw] = jnp.dot(scaled, wqkv[...], preferred_element_type=F32)
+    gain = gain1_v[:, pl.ds(offset, width)]
     wf = wf_v[:, pl.ds(offset, width)].astype(F32)
-    scaled32 = scaled.astype(F32)
-    extra = jnp.broadcast_to(squares, (rows, 128))
-    bias_rows = []
+    bias_rows, forget_rows = [], []
     for h in range(local_heads):
         picked = wf[h : h + 1]
         bias_h = bias_v[:, h : h + 1]
@@ -162,9 +160,31 @@
             picked = jnp.where(tp == t, wf[g : g + 1], picked)
             bias_h = jnp.where(tp == t, bias_v[:, g : g + 1], bias_h)
         bias_rows.append(bias_h)
-        gate = jnp.sum(scaled32 * picked, axis=1, keepdims=True)
-        extra = jnp.where(lane == h, gate, extra)
-    proj[kv, :rows, qw + 2 * kw :] = extra
+        forget_rows.append(picked)
+
+    def project(which):
+        block = halves[which].astype(F32)
+        scaled = (block * part(gain, which)).astype(BF16)
+        start = pl.multiple_of(which * half, half)
+        product = jnp.dot(scaled, wqkv[pl.ds(start, half), :], preferred_element_type=F32)
+        extra = jnp.broadcast_to(jnp.sum(block * block, axis=1, keepdims=True), (rows, 128))
+        for h in range(local_heads):
+            gate = jnp.sum(
+                scaled.astype(F32) * part(forget_rows[h], which), axis=1, keepdims=True
+            )
+            extra = jnp.where(slot == h, gate, extra)
+        return product, extra
+
+    load_wq.wait()
+    load_wk.wait()
+    load_wv.wait()
+    product, extra = project(tp)
+    swap.wait_recv()
+    product_b, extra_b = project(peer)
+    proj[kv, :rows, : qw + 2 * kw] = (product + product_b).astype(BF16)
+    extra = extra + extra_b
+    coarse = extra.astype(BF16).astype(F32)
+    proj[kv, :rows, qw + 2 * kw :] = jnp.where(lane < HEAD, coarse, extra - coarse).astype(BF16)
 
     copies = to_all(0, proj.at[kv])
     load_keys.wait()
@@ -172,10 +192,11 @@
     load_values.wait()
     for copy in copies:
         copy.wait_recv()
-    total = proj[0, :rows, :]
+    total = proj[0, :rows, :].astype(F32)
     for i in range(1, n_kv):
-        total = total + proj[i, :rows, :]
+        total = total + proj[i, :rows, :].astype(F32)
     extra = total[:, qw + 2 * kw :]
+    extra = extra + pltpu.roll(extra, HEAD, 1)
     inverse = lax.rsqrt(extra[:, local_heads : local_heads + 1] / features + EPS)
     query = (total[:, :qw] * inverse).astype(BF16).astype(F32) * (HEAD ** (-0.5))
     key_new = (total[:, qw : qw + kw] * inverse).astype(BF16).astype(F32)
@@ -202,7 +223,15 @@
     def both(pair):
         return jnp.where(low, pair[:group], pair[group:])
 
-    front = jnp.bitwise_and(lane, HEAD - 1) < HEAD // 2
+    quarter = HEAD // 4
+    front = slot < 2 * quarter
+    even = jnp.bitwise_and(lane, 2 * quarter - 1) < quarter
+    outcomes, stats = [], []
+
+    def split(value):
+        coarse = value.astype(BF16).astype(F32)
+        return coarse, (value - coarse).astype(BF16).astype(F32)
+
     for b in range(rows):
         q_b = qs[b * per_row : (b + 1) * per_row, :].astype(BF16)
         scores = lax.dot_general(
@@ -217,37 +246,50 @@
             axis=0,
         )
         maxima = jnp.max(scores, axis=1, keepdims=True)
-        weights = jnp.exp(scores - maxima)
+        high, low_part = split(maxima)
+        weights = jnp.exp(scores - (high + low_part))
         totals = jnp.sum(weights, axis=1, keepdims=True)
         mixed = jnp.dot(weights.astype(BF16), values_v[b], preferred_element_type=F32)
-        peak = both(maxima) + jnp.where(low, forget[0][b : b + 1], forget[1][b : b + 1])
-        soft[kv, 0, b * group : (b + 1) * group, :] = both(mixed)
-        soft[kv, 1, b * group : (b + 1) * group, :] = jnp.where(front, peak, both(totals))
+        outcomes.append(both(mixed))
+        count_high, count_low = split(totals)
+        peak_tile = jnp.where(even, both(high), both(low_part))
+        count_tile = jnp.where(even, both(count_high), both(count_low))
+        stats.append(jnp.where(front, peak_tile, count_tile))
+    soft[kv] = jnp.concatenate(outcomes + stats, axis=0).astype(BF16)
     copies = to_all(1, soft.at[kv])
     fresh, fresh_value = [], []
     for b in range(rows):
         q_b = qs[b * per_row : (b + 1) * per_row, :]
-        fresh.append(both(jnp.sum(q_b * key_new[b : b + 1], axis=1, keepdims=True)))
+        own_score = both(jnp.sum(q_b * key_new[b : b + 1], axis=1, keepdims=True))
+        own_gate = jnp.where(low, forget[0][b : b + 1], forget[1][b : b + 1])
+        fresh.append(own_score - own_gate)
         fresh_value.append(jnp.broadcast_to(value_new[b : b + 1], (group, 128)))
     fresh = jnp.concatenate(fresh, axis=0)
     fresh_value = jnp.concatenate(fresh_value, axis=0)
     for copy in copies:
         copy.wait_recv()
-    peaks, counts = [], []
+    peaks, counts, partial = [], [], []
+    cells = rows * group
     for i in range(n_kv):
-        stat = soft[i, 1]
-        peaks.append(jnp.where(front, stat, pltpu.roll(stat, HEAD // 2, 1)))
-        counts.append(jnp.where(front, pltpu.roll(stat, 128 - HEAD // 2, 1), stat))
+        message = soft[i].astype(F32)
+        partial.append(message[:cells])
+        stat = message[cells:]
+        stat = stat + jnp.where(
+            even, pltpu.roll(stat, 128 - quarter, 1), pltpu.roll(stat, quarter, 1)
+        )
+        counts.append(stat)
+        peaks.append(jnp.where(front, stat, pltpu.roll(stat, 2 * quarter, 1)))
     peak = fresh
     for item in peaks:
         peak = jnp.maximum(peak, item)
     own = jnp.exp(fresh - peak)
-    count = own
+    count = 0.0
     mixed = own.astype(BF16).astype(F32) * fresh_value
     for i in range(n_kv):
         scale = jnp.exp(peaks[i] - peak)
         count = count + counts[i] * scale
-        mixed = mixed + soft[i, 0] * scale
+        mixed = mixed + partial[i] * scale
+    count = jnp.where(front, pltpu.roll(count, 128 - 2 * quarter, 1), count) + own
     att[...] = mixed / count
     blocks = [[] for _ in range(local_heads)]
     for t in range(group // 2):
@@ -268,6 +310,7 @@
     load_gain2.wait()
     load_wu.wait()
     swap.wait_recv()
+    source = jnp.concatenate([halves[t].astype(F32) for t in range(n_tp)], axis=1)
     added = branch[0, :rows, :].astype(F32)
     for t in range(1, n_tp):
         added = added + branch[t, :rows, :].astype(F32)
@@ -301,12 +344,6 @@
             hidden, wd_v[c * ff_chunk : (c + 1) * ff_chunk, :], preferred_element_type=F32
         )
 
-    def part(value, which):
-        picked = value[:, :half]
-        for t in range(1, n_tp):
-            picked = jnp.where(which == t, value[:, t * half : (t + 1) * half], picked)
-        return picked
-
     tail_out[:rows, :] = part(down, peer).astype(BF16)
     swap = to_peer(2, tail_out, tail_in)
     kept = part(down, tp).astype(BF16).astype(F32)
@@ -348,7 +385,7 @@
     exchanges = 3 + CHUNKS
     return pl.pallas_call(
         functools.partial(layer_kernel, n_kv, n_tp),
-        out_shape=jax.ShapeDtypeStruct((rows, half), BF16),
+        out_shape=pltpu.VMEM((rows, half), BF16),
         in_specs=[pl.BlockSpec(memory_space=pl.ANY)] * 14,
         out_specs=pl.BlockSpec(memory_space=pltpu.VMEM),
         scratch_shapes=[
@@ -364,9 +401,9 @@
             pltpu.VMEM(gain2.shape, F32),
             pltpu.VMEM(w_up.shape, BF16),
             pltpu.VMEM(w_down.shape, BF16),
-            pltpu.VMEM((n_kv, padded, qw + 2 * kw + 128), F32),
+            pltpu.VMEM((n_kv, padded, qw + 2 * kw + 128), BF16),
             pltpu.VMEM((rows * local_heads * group, 128), F32),
-            pltpu.VMEM((n_kv, 2, rows * group, 128), F32),
+            pltpu.VMEM((n_kv, 2 * rows * group, 128), BF16),
             pltpu.VMEM((rows * group, 128), F32),
             pltpu.VMEM((n_tp, padded, width), BF16),
             pltpu.VMEM((n_kv, padded, 128), F32),

time: 25.1 us -> 22.9 us (0.912)
  Pallas kernels: 23.6 us -> 22.1 us
  local copies, waits for them, and re-layouts: 1.26 us -> 0.58 us
    pallas_call x1, Pallas kernels: 23.6 us -> 22.1 us  [layer(): pl.pallas_call(functools.partial(layer_kernel, n_kv, n_tp), out_shape=plt...]
    unnamed x1, local copies, waits for them, and re-layouts: 1.26 us -> 0.58 us
where the time goes in v2:
time: 22.9 us; the launch traced here: 22.7 us
  Pallas kernels  22.1 us (97%)
  local copies, waits for them, and re-layouts  0.58 us (3%)
    pallas_call x1, Pallas kernels, layer(): pl.pallas_call(functools.partial(layer_kernel, n_kv, n_tp), out_shape=plt...  22.1 us
    unnamed x1, local copies, waits for them, and re-layouts  0.58 us

profile of v2, /device:TPU:0, one launch (start us, length us, event | category | flops | bytes accessed | tf_op | source)
XLA Modules:
  0.0 22.7 jit_solution(7858233316160399760)
XLA Ops:
  0.0 22.1 %shard_map.136 = bf16[3,256]{1,0:T(4,128)(2,1)S(1)} custom-call(bf16[3,256]{1,0:T(4,128)(2,1)} %resid.1, bf16[3,1024,128]{2,1,0:T(8,128)(2,1)} %keys.1, bf16[3,1024,128]{2,1,0:T(8,128)(2,1)} %values.1, f32[3,2,1024]{2,1,0:T(2,128)} %bitcast.5, f32[1,2048]{1,0:T(1,128)} %bitcast.7, bf16[512,1024]{1,0:T(8,128)(2,1)} %w_query.1, bf16[512,128]{1,0:T(8,128)(2,1)} %w_key.1, ...), custom_call_target="tpu_custom_call" | custom-call | tf_op jit(solution)/shard_map/pallas_call | solution.py:386
  22.2 0.6 %copy.16 = bf16[3,256]{1,0:T(4,128)(2,1)} copy(bf16[3,256]{1,0:T(4,128)(2,1)S(1)} %shard_map.136) | data formatting | bytes 3072
